TPU v7x, 32 devices: a whole 2x2x4 slice. The times are simulated.
32 devices in a mesh: dp: 4 (over y, x), kv: 4 (over z), tp: 2 (over core).
Axes of the slice: x: 2, y: 2, z: 4, core: 2. Of those that a mesh axis runs over, the one named last changes fastest.
Arguments:
- tokens: bfloat16 [16, 4096], P('dp', ('kv', 'tp')), may hold values from -11 to 11
- attn_gain: float32 [4096], replicated, may hold values from 0.1 to 1.9
- query_weight: bfloat16 [4096, 4096], P('kv', 'tp'), may hold values from -0.09375 to 0.09375
- key_cache: bfloat16 [16, 1024, 2, 128], P('dp', 'kv', 'tp'), may hold values from -820 to 820
- value_cache: bfloat16 [16, 1024, 2, 128], P('dp', 'kv', 'tp'), may hold values from -6 to 6
- head_lambda: float32 [32], P('tp'), may hold values from 0.3 to 0.8
- head_gain: float32 [128], replicated, may hold values from 0.1 to 1.9
- out_weight: bfloat16 [4096, 4096], P('kv', 'tp'), may hold values from -0.09375 to 0.09375
- mlp_gain: float32 [4096], replicated, may hold values from 0.1 to 1.9
- gate_weight: bfloat16 [11264, 4096], P(('kv', 'tp')), may hold values from -0.09375 to 0.09375
- up_weight: bfloat16 [11264, 4096], P(('kv', 'tp')), may hold values from -0.09375 to 0.09375
- down_weight: bfloat16 [11264, 4096], P(('kv', 'tp')), may hold values from -0.078125 to 0.078125
Outputs:
- mixed: bfloat16 [16, 4096], P('dp', ('kv', 'tp'))
All inputs are finite; a program needn't handle non-finite values.
Results may differ from a plain program's by a relative error of at most 0.02.
The roundings to bfloat16 on the way count: a program that leaves them out, or rounds other values in their place, can miss the bound.
Values may be sent and summed in bfloat16 or wider, within the bound.
A program may use at most 128 MiB of HBM per device.

v0:
```python
import jax
import jax.numpy as jnp
from jax import lax
from jax.sharding import PartitionSpec as P

EPS = 1e-06
THETA = 10000.0


def merged(x, axis, combine):
    everything = jax.tree.map(lambda part: lax.all_gather(part, axis), x)
    first = jax.tree.map(lambda part: part[0], everything)

    def hop(k, so_far):
        return combine(so_far, jax.tree.map(lambda part: part[k], everything))

    return lax.fori_loop(1, lax.axis_size(axis), hop, first)


def rotate(vector, position):
    half_len = vector.shape[-1] // 2
    inv_freq = 1.0 / THETA ** (jnp.arange(half_len, dtype=jnp.float32) / half_len)
    angles = position * inv_freq
    cos_table = jnp.cos(angles)
    sin_table = jnp.sin(angles)
    first_half = vector[..., :half_len]
    second_half = vector[..., half_len:]
    return jnp.concatenate(
        [
            first_half * cos_table - second_half * sin_table,
            second_half * cos_table + first_half * sin_table,
        ],
        axis=-1,
    )


def combine(earlier, latter):
    peak_a, total_a, value_a = earlier
    peak_b, total_b, value_b = latter
    peak_new = jnp.maximum(peak_a, peak_b)
    factor_a = jnp.exp(peak_a - peak_new)
    factor_b = jnp.exp(peak_b - peak_new)
    return (
        peak_new,
        total_a * factor_a + total_b * factor_b,
        value_a * factor_a[..., None] + value_b * factor_b[..., None],
    )


def inner_last(left, right):
    return lax.dot_general(
        left, right, (((1,), (1,)), ((), ())), preferred_element_type=jnp.float32
    )


def shards(
    tokens,
    attn_gain,
    query_weight,
    key_cache,
    value_cache,
    head_lambda,
    head_gain,
    out_weight,
    mlp_gain,
    gate_weight,
    up_weight,
    down_weight,
):
    row_count = tokens.shape[0]
    kv_count = lax.axis_size("kv")
    tp_count = lax.axis_size("tp")
    kv_index = lax.axis_index("kv")
    row_span = query_weight.shape[0]
    full_rows = lax.all_gather(tokens, ("kv", "tp"), axis=1, tiled=True)
    wide_rows = full_rows.astype(jnp.float32)
    mean_square = jnp.mean(wide_rows * wide_rows, axis=-1, keepdims=True)
    scaled = (wide_rows * attn_gain).astype(jnp.bfloat16)
    local_cols = lax.dynamic_slice_in_dim(scaled, kv_index * row_span, row_span, 1)
    queries = lax.psum(jnp.dot(local_cols, query_weight, preferred_element_type=jnp.float32), "kv")
    queries = queries * lax.rsqrt(mean_square + EPS)
    head_count = head_lambda.shape[0]
    kv_local = key_cache.shape[2]
    group_size = head_count // kv_local
    position_count = key_cache.shape[1]
    half_dim = key_cache.shape[3] // 2
    value_dim = value_cache.shape[3]
    queries = queries.reshape(row_count, kv_local, group_size, 2, half_dim)
    rotated = rotate(queries, jnp.float32(position_count * kv_count)).astype(jnp.bfloat16)
    key_grid = key_cache.reshape(row_count, position_count, kv_local, 2, half_dim)
    scores = jnp.einsum(
        "bkgch,bpkch->bkgcp", rotated, key_grid, preferred_element_type=jnp.float32
    ) * half_dim ** (-0.5)
    local_peak = jnp.max(scores, axis=-1)
    weights_exp = jnp.exp(scores - local_peak[..., None])
    lam_grid = head_lambda.reshape(kv_local, group_size)[None, :, :, None]
    exp_total = jnp.sum(weights_exp, axis=-1)
    weighted = jnp.einsum(
        "bkgcp,bpkv->bkgcv",
        weights_exp.astype(jnp.bfloat16),
        value_cache,
        preferred_element_type=jnp.float32,
    )
    peak_all, total_all, weighted_all = merged((local_peak, exp_total, weighted), "kv", combine)
    attended = weighted_all / total_all[..., None]
    difference = attended[:, :, :, 0] - lam_grid * attended[:, :, :, 1]
    head_norm = lax.rsqrt(jnp.mean(difference * difference, axis=-1, keepdims=True) + EPS)
    head_out = (difference * head_norm * head_gain).reshape(row_count, head_count * value_dim)
    head_out = head_out.astype(jnp.bfloat16)
    out_part = inner_last(head_out, out_weight).astype(jnp.bfloat16)
    pieces = lax.all_gather(out_part, ("kv", "tp"), axis=1, tiled=True)
    attention = jnp.sum(
        pieces.astype(jnp.float32).reshape(row_count, kv_count, tp_count, -1), axis=2
    )
    stream = wide_rows + attention.reshape(row_count, -1)
    stream_square = jnp.mean(stream * stream, axis=-1, keepdims=True)
    normed = (stream * lax.rsqrt(stream_square + EPS) * mlp_gain).astype(jnp.bfloat16)
    gate_out = inner_last(normed, gate_weight)
    up_out = inner_last(normed, up_weight)
    hidden = (jax.nn.silu(gate_out) * up_out).astype(jnp.bfloat16)
    own_cols = tokens.shape[1]
    down_cols = lax.psum_scatter(
        lax.dot_general(
            down_weight, hidden, (((0,), (1,)), ((), ())), preferred_element_type=jnp.float32
        ),
        ("kv", "tp"),
        scatter_dimension=0,
        tiled=True,
    )
    column_index = lax.axis_index(("kv", "tp"))
    own_stream = lax.dynamic_slice_in_dim(stream, column_index * own_cols, own_cols, 1)
    return (own_stream + down_cols.T).astype(jnp.bfloat16)


def solution(mesh):
    placed = (
        P("dp", ("kv", "tp")),
        P(),
        P("kv", "tp"),
        P("dp", "kv", "tp", None),
        P("dp", "kv", "tp", None),
        P("tp"),
        P(),
        P("kv", "tp"),
        P(),
        P(("kv", "tp"), None),
        P(("kv", "tp"), None),
        P(("kv", "tp"), None),
    )
    return jax.shard_map(
        shards, mesh=mesh, in_specs=placed, out_specs=P("dp", ("kv", "tp")), check_vma=False
    )
```

profile of v0, /device:TPU:0, one launch (start us, length us, event | category | flops | bytes accessed | tf_op | source)
XLA Modules:
  0.0 174.8 jit_solution(18211081603374281801)
XLA Ops:
  6.5 0.0 copy-start
  6.5 0.0 copy-start.1
  6.5 0.0 reduce-scatter.4.cloned.1.call-start
  6.6 16.1 %all_gather.24 = bf16[4,4096]{1,0:T(4,128)(2,1)S(1)} all-gather(bf16[4,512]{1,0:T(4,128)(2,1)} %param.14), channel_id=1, replica_groups=mesh['dp'=4,'kv'=4,'tp'=2] {'kv','tp'}, dimensions={1}, use_global_device_ids=true | all-gather | bytes 36864 | tf_op jit(solution)/shard_map/all_gather | solution.py:75
  22.7 0.1 multiply_reduce_fusion.1
  22.8 0.7 dynamic-slice
  23.5 2.8 %fusion.32 = f32[4,2048]{1,0:T(4,128)S(1)} fusion(bf16[1024,2048]{1,0:T(8,128)(2,1)} %param.16, f32[4,4096]{1,0:T(4,128)S(1)} %convert_element_type.29, s32[]{:T(128)S(6)} %select_n.18, f32[1024]{0:T(1024)S(1)} %dynamic-slice), kind=kOutput, calls=%fused_computation.58 | convolution fusion | flops 16785408 | bytes 4247556 | tf_op jit(solution)/shard_map/dot_general | solution.py:80
  26.4 19.0 %psum.7 = f32[4,2048]{1,0:T(4,128)S(1)} all-reduce(f32[4,2048]{1,0:T(4,128)S(1)} %fusion.32), channel_id=1, replica_groups=mesh['dp'=4,'kv'=4,'tp'=2] {'kv'}, use_global_device_ids=true, to_apply=%region_0.0 | all-reduce | flops 8192 | bytes 65536 | tf_op jit(solution)/shard_map/psum | solution.py:80
  45.4 0.1 broadcast_multiply_fusion
  45.4 0.1 reshape.176
  45.6 0.1 fusion.43
  45.7 1.1 copy.39
  46.8 0.3 fusion.44
  47.1 13.2 %all-gather = f32[16,16,2]{1,2,0:T(2,128)S(1)} all-gather(f32[4,16,2]{1,2,0:T(2,128)S(1)} %get-tuple-element.234), channel_id=2, replica_groups=mesh['dp'=4,'kv'=4,'tp'=2] {'kv'}, dimensions={0}, use_global_device_ids=true | all-gather | bytes 2560 | tf_op jit(solution)/shard_map/all_gather | solution.py:11
  60.3 0.2 fusion.12
  60.5 0.0 copy-done
  60.5 0.2 fusion.9
  60.8 13.2 %all-gather.1 = f32[16,16,2]{1,2,0:T(2,128)S(1)} all-gather(f32[4,16,2]{1,2,0:T(2,128)S(1)} %fusion.12), channel_id=3, replica_groups=mesh['dp'=4,'kv'=4,'tp'=2] {'kv'}, dimensions={0}, use_global_device_ids=true | all-gather | bytes 2560 | tf_op jit(solution)/shard_map/all_gather | solution.py:11
  74.0 13.8 %all-gather.2 = f32[16,16,2,128]{3,1,2,0:T(8,128)S(1)} all-gather(f32[4,16,2,128]{3,1,2,0:T(8,128)S(1)} %fusion.9), channel_id=4, replica_groups=mesh['dp'=4,'kv'=4,'tp'=2] {'kv'}, dimensions={0}, use_global_device_ids=true | all-gather | bytes 327680 | tf_op jit(solution)/shard_map/all_gather | solution.py:11
  87.8 2.1 %while.19 = (s32[]{:T(128)}, f32[4,1,16,2]{2,0,3,1:T(4,128)S(1)}, f32[4,1,16,2]{2,0,3,1:T(4,128)S(1)}, f32[4,1,16,2,128]{4,3,2,1,0:T(2,128)S(1)}, f32[4,4,1,16,2...) while((s32[]{:T(128)}, f32[4,1,16,2]{2,0,3,1:T(4,128)S(1)}, ...), condition=%wide.region_5.0_spmd, body=%wide.region_4.0_spmd.sunk | while | flops 50053 | bytes 339599 | solution.py:17
  87.9 0.1 copy.116
  88.0 0.1 copy.115
  88.1 0.4 fusion.56
  88.6 0.1 copy.116
  88.7 0.1 copy.115
  88.8 0.4 fusion.56
  89.4 0.1 copy.116
  89.5 0.1 copy.115
  89.6 0.4 fusion.56
  90.0 0.1 copy.48
  90.1 0.1 broadcast_divide_fusion
  90.2 0.1 slice_reduce_fusion
  90.4 0.7 broadcast_bitcast_fusion.1
  91.1 0.8 multiply_reduce_fusion.2
  91.9 0.1 broadcast_bitcast_fusion
  92.0 3.4 %convolution_convert_fusion = bf16[4,1024]{1,0:T(4,128)(2,1)S(1)} fusion(bf16[1024,2048]{1,0:T(8,128)(2,1)} %param.21, f32[1,4,16,128]{3,2,1,0:T(8,128)S(1)} %broadcast_bitcast_fusion, f32[1,4,16,128]{3,2,1,0:T(8,128)S(1)} %bitcast.122, f32[1,4,16,128]{3,2,1,0:T(8,128)S(1)} %bitcast.117, f32[2048]{0:T(1024)S(1)} %get-tuple-element.238, ...), kind=kOutput, calls=%fused_computation.20 | convolution fusion | flops 16822272 | bytes 4317184 | tf_op jit(solution)/shard_map/dot_general | solution.py:51
  95.4 14.2 %all_gather.31 = bf16[4,8192]{1,0:T(4,128)(2,1)S(1)} all-gather(bf16[4,1024]{1,0:T(4,128)(2,1)S(1)} %convolution_convert_fusion), channel_id=1, replica_groups=mesh['dp'=4,'kv'=4,'tp'=2] {'kv','tp'}, dimensions={1}, use_global_device_ids=true | all-gather | bytes 73728 | tf_op jit(solution)/shard_map/all_gather | solution.py:111
  109.6 0.1 reshape.184
  109.7 0.2 reduce_sum.48
  109.9 0.1 multiply_reduce_fusion
  110.0 0.0 copy-done.1
  110.1 7.3 %fusion.41 = f32[4,1408]{1,0:T(4,128)S(1)} fusion(bf16[1408,4096]{1,0:T(8,128)(2,1)} %param.23, f32[4,4096]{1,0:T(4,128)S(1)} %get-tuple-element.222, f32[4096]{0:T(1024)S(1)} %copy-done.1, f32[4]{0:T(128)S(1)} %add_rsqrt_fusion.1), kind=kOutput, calls=%fused_computation.76 | convolution fusion | flops 46186496 | bytes 11638800 | tf_op jit(solution)/shard_map/dot_general | solution.py:51
  117.4 12.5 %convolution_bitcast_fusion = f32[4096,4]{0,1:T(4,128)S(1)} fusion(bf16[1408,4096]{1,0:T(8,128)(2,1)} %param.25, bf16[1408,4096]{1,0:T(8,128)(2,1)} %param.24, f32[4,1408]{1,0:T(4,128)S(1)} %fusion.41, f32[4,4096]{1,0:T(4,128)S(1)} %get-tuple-element.222, f32[4096]{0:T(1024)S(1)} %copy-done.1, f32[4]{0:T(128)S(1)} %add_rsqrt_fusion.1), kind=kOutput, calls=%fused_computation.15 | convolution fusion | flops 92357632 | bytes 23238672 | tf_op jit(solution)/shard_map/dot_general | solution.py:123
  129.9 2.0 %copy.55 = f32[4096,4]{1,0:T(8,128)} copy(f32[4096,4]{0,1:T(4,128)S(1)} %convolution_bitcast_fusion) | data formatting | bytes 131072
  131.9 0.0 reduce-scatter.4.cloned.1.call-update
  131.9 34.3 %reduce-scatter.4.cloned.1.call-done = f32[512,4]{1,0:T(8,128)} async-done(((f32[4096,4]{1,0:T(8,128)}), f32[512,4]{1,0:T(8,128)}) %reduce-scatter.4.cloned.1.call-update) | async-done | bytes 8208
  166.3 1.1 copy.56
  167.3 0.6 fusion.35
  (28 shorter events, 0.3 us)
Async XLA Ops:
  6.5 54.0 %copy-start = (bf16[4,256,1,128]{3,1,2,0:T(8,128)(2,1)S(1)}, bf16[4,256,1,128]{3,1,2,0:T(8,128)(2,1)}, u32[]{:S(2)}) copy-start(bf16[4,256,1,128]{3,1,2,0:T(8,128)(2,1)} %param.18) | copy-start | bytes 786436
  6.5 103.5 %copy-start.1 = (f32[4096]{0:T(1024)S(1)}, f32[4096]{0:T(1024)}, u32[]{:S(2)}) copy-start(f32[4096]{0:T(1024)} %param.22) | copy-start | bytes 49156
  6.5 159.7 %reduce-scatter.4.cloned.1.call-start = ((), (), s32[]{:S(2)}) async-start(), calls=%async_computation.1 | async-start | bytes 2359296
Sparse Core Ops, SparseCore 0:
  132.0 34.1 reduce-scatter.3
where the time goes:
time: 175 us
  blocking collectives  89.4 us (51%)
  waiting for transfers between devices  34.3 us (20%)
  matrix products  26.6 us (15%)
  between operations  13.6 us (8%)
  local copies, waits for them, and re-layouts  6.98 us (4%)
  other arithmetic  3.75 us (2%)
    all_gather x3, blocking collectives, merged(): everything = jax.tree.map(lambda part: lax.all_gather(part, axis), x)  40.2 us
    unnamed x2, waiting for transfers between devices  34.3 us
    psum x1, blocking collectives, shards(): lax.psum(jnp.dot(local_cols, query_weight, preferred_element_type=jnp.flo...  19 us
    all_gather x1, blocking collectives, shards(): full_rows = lax.all_gather(tokens, ('kv', 'tp'), axis=1, tiled=True)  16.1 us
    all_gather x1, blocking collectives, shards(): pieces = lax.all_gather(out_part, ('kv', 'tp'), axis=1, tiled=True)  14.2 us
    dot_general x1, matrix products, shards(): lax.dot_general(down_weight, hidden, (((0,), (1,)), ((), ())), preferred_...  12.5 us
    dot_general x2, matrix products, inner_last(): lax.dot_general(left, right, (((1,), (1,)), ((), ())), preferred_element_...  10.7 us
    unnamed x9, local copies, waits for them, and re-layouts  4.29 us
  transfers between devices with their start and end apart: 1, of which 1 were waited for; matrix products, arithmetic and copies ran while one was open for 0% of the time, Pallas kernels for 0%

commit v1 on v0

--- a/solution.py
+++ b/solution.py
@@ -1,10 +1,16 @@
+import functools
+
 import jax
 import jax.numpy as jnp
+import numpy as np
 from jax import lax
+from jax.experimental import pallas as pl
+from jax.experimental.pallas import tpu as pltpu
 from jax.sharding import PartitionSpec as P
 
 EPS = 1e-06
 THETA = 10000.0
+LANES = 128
 
 
 def merged(x, axis, combine):
@@ -132,6 +138,350 @@
     return (own_stream + down_cols.T).astype(jnp.bfloat16)
 
 
+def same_chip_kernel(
+    kv_n, tp_n, tok, again, wq_h, kc_h, vc_h, lam, hgain, wo_h, mgain, wg_h, wu_h, wd_h, table,
+    out,
+    wq, kc, vc, wo, wg, wu, wd,
+    tg, qs, qr, qf, ms, mr, hs, ho, hf, og, og_r, stream, hid, ds, dr,
+    wsem, tsend, trecv, qsend, qrecv, msend, mrecv, hsend, hrecv, osend, orecv, dsend, drecv,
+):
+    kv, tp = lax.axis_index("kv"), lax.axis_index("tp")
+    n_all = kv_n * tp_n
+    me = kv * tp_n + tp
+    rows, own = tok.shape
+    loads = []
+    for slot, (src, dst) in enumerate(
+        [(wq_h, wq), (kc_h, kc), (vc_h, vc), (wo_h, wo), (wg_h, wg), (wu_h, wu), (wd_h, wd)]
+    ):
+        load = pltpu.make_async_copy(src, dst, wsem.at[slot])
+        load.start()
+        loads.append(load)
+
+    def spot(delta):
+        other = lax.rem(me + delta, n_all)
+        return {"kv": other // tp_n, "tp": lax.rem(other, tp_n)}
+
+    def along(delta):
+        return {"kv": lax.rem(kv + delta, kv_n), "tp": tp}
+
+    def remote(src, dst, send, recv, where):
+        copy = pltpu.make_async_remote_copy(
+            src_ref=src, dst_ref=dst, send_sem=send, recv_sem=recv,
+            device_id=where, device_id_type=pl.DeviceIdType.MESH,
+        )
+        copy.start()
+        return copy
+
+    barrier = pltpu.get_barrier_semaphore()
+    for delta in range(1, n_all):
+        pl.semaphore_signal(
+            barrier, inc=1, device_id=spot(delta), device_id_type=pl.DeviceIdType.MESH
+        )
+    tg[me] = tok[...]
+    pl.semaphore_wait(barrier, n_all - 1)
+    sends = []
+
+    mate = {"kv": kv, "tp": lax.rem(tp + 1, tp_n)}
+    pair = remote(tok, tg.at[me], tsend.at[0], trecv.at[0], mate)
+    token_copies = [pair]
+    for delta in range(1, kv_n):
+        for across in range(tp_n):
+            where = {"kv": lax.rem(kv + delta, kv_n), "tp": lax.rem(tp + across, tp_n)}
+            slot = delta * tp_n + across
+            token_copies.append(remote(tok, tg.at[me], tsend.at[slot], trecv.at[slot], where))
+    sends += token_copies
+
+    pair.wait_recv()
+    parts = []
+    for half in range(tp_n):
+        at = kv * tp_n + half
+        gain = again[:, pl.ds(pl.multiple_of(at * own, LANES), own)]
+        parts.append((tg[at].astype(jnp.float32) * gain).astype(jnp.bfloat16))
+    scaled = jnp.concatenate(parts, axis=1)
+    loads[0].wait()
+    head_count = qs.shape[0]
+    value_dim = qs.shape[2]
+    per = 4
+    pieces = head_count // per
+    query_copies = []
+    for j in range(pieces):
+        width = per * value_dim
+        product = jnp.dot(
+            scaled, wq[:, j * width:(j + 1) * width], preferred_element_type=jnp.float32
+        )
+        for i in range(per):
+            qs[j * per + i] = product[:, i * value_dim:(i + 1) * value_dim]
+        for delta in range(1, kv_n):
+            part = pl.ds(j * per, per)
+            query_copies.append(
+                remote(
+                    qs.at[part], qr.at[delta - 1, part],
+                    qsend.at[j, delta - 1], qrecv.at[j, delta - 1], along(delta),
+                )
+            )
+    sends += query_copies
+
+    for copy in token_copies[1:]:
+        copy.wait_recv()
+    square = jnp.zeros((rows, 1), jnp.float32)
+    for at in range(n_all):
+        wide = tg[at].astype(jnp.float32)
+        square = square + jnp.sum(wide * wide, axis=1, keepdims=True)
+    scale = lax.rsqrt(square / (n_all * own) + EPS)
+
+    for copy in query_copies:
+        copy.wait_recv()
+    lane = lax.broadcasted_iota(jnp.int32, (rows, value_dim), 1)
+    half = value_dim // 2
+    first = lax.rem(lane, half) < half // 2
+    cosines = table[0:1, :]
+    sines = table[1:2, :]
+    for h in range(head_count):
+        total = qs[h]
+        for delta in range(1, kv_n):
+            total = total + qr[delta - 1, h]
+        total = total * scale
+        swapped = jnp.where(
+            first,
+            pltpu.roll(total, value_dim - half // 2, 1),
+            pltpu.roll(total, half // 2, 1),
+        )
+        qf[h] = total * cosines + swapped * sines
+
+    loads[1].wait()
+    loads[2].wait()
+    both = 2 * head_count
+    low = lax.broadcasted_iota(jnp.int32, (head_count, value_dim), 1) < half
+    row_at = lax.broadcasted_iota(jnp.int32, (both, value_dim), 0)
+    lane_at = lax.broadcasted_iota(jnp.int32, (both, value_dim), 1)
+    for b in range(rows):
+        query = qf[:, b, :]
+        grid = jnp.concatenate(
+            [jnp.where(low, query, 0.0), jnp.where(low, 0.0, query)], axis=0
+        ).astype(jnp.bfloat16)
+        scores = inner_last(grid, kc[b]) * half ** (-0.5)
+        peak = jnp.max(scores, axis=1, keepdims=True)
+        exps = jnp.exp(scores - peak)
+        sums = jnp.sum(exps, axis=1, keepdims=True)
+        ms[b, 0:both, :] = jnp.dot(
+            exps.astype(jnp.bfloat16), vc[b], preferred_element_type=jnp.float32
+        )
+        stats = jnp.where(lane_at == row_at, peak, 0.0) + jnp.where(
+            lane_at == row_at + both, sums, 0.0
+        )
+        ms[b, both:both + 8, :] = jnp.broadcast_to(
+            jnp.sum(stats, axis=0, keepdims=True), (8, value_dim)
+        )
+
+    merge_copies = []
+    for delta in range(1, kv_n):
+        other = lax.rem(kv + delta, kv_n)
+        merge_copies.append(
+            remote(
+                ms.at[other], mr.at[delta - 1],
+                msend.at[delta - 1], mrecv.at[delta - 1], along(delta),
+            )
+        )
+    sends += merge_copies
+
+    lam_at = lax.broadcasted_iota(jnp.int32, (head_count, head_count), 0)
+    lam_lane = lax.broadcasted_iota(jnp.int32, (head_count, head_count), 1)
+    lam_col = jnp.sum(
+        jnp.where(lam_at == lam_lane, lam[...], 0.0), axis=1, keepdims=True
+    )
+    for copy in merge_copies:
+        copy.wait_recv()
+    gathered = []
+    for source in range(kv_n):
+        block = ms[kv] if source == 0 else mr[source - 1]
+        stats = block[both:both + 1, :]
+        peak = jnp.sum(jnp.where(lane_at == row_at, stats, 0.0), axis=1, keepdims=True)
+        sums = jnp.sum(jnp.where(lane_at == row_at + both, stats, 0.0), axis=1, keepdims=True)
+        gathered.append((peak, sums, block[0:both, :]))
+    top = gathered[0][0]
+    for peak, _, _ in gathered[1:]:
+        top = jnp.maximum(top, peak)
+    all_sums = jnp.zeros_like(top)
+    weighted = jnp.zeros((both, value_dim), jnp.float32)
+    for peak, sums, values in gathered:
+        factor = jnp.exp(peak - top)
+        all_sums = all_sums + sums * factor
+        weighted = weighted + values * factor
+    attended = weighted / all_sums
+    difference = attended[0:head_count] - lam_col * attended[head_count:both]
+    norm = lax.rsqrt(jnp.mean(difference * difference, axis=1, keepdims=True) + EPS)
+    head_out = (difference * norm * hgain[...]).astype(jnp.bfloat16)
+    hs[...] = head_out
+    ho[kv] = head_out
+    head_copies = []
+    for delta in range(1, kv_n):
+        head_copies.append(
+            remote(hs, ho.at[kv], hsend.at[delta - 1], hrecv.at[delta - 1], along(delta))
+        )
+    sends += head_copies
+    for copy in head_copies:
+        copy.wait_recv()
+    for b in range(rows):
+        hf[b] = ho[b].astype(jnp.float32)
+    flat = jnp.concatenate(
+        [hf[:, h, :] for h in range(head_count)], axis=1
+    ).astype(jnp.bfloat16)
+    loads[3].wait()
+    features = wo.shape[0]
+    width = 256
+    for j in range(features // width):
+        part = inner_last(flat, wo[j * width:(j + 1) * width, :]).astype(jnp.bfloat16)
+        og[:, j * width:(j + 1) * width] = part
+    og_r[me] = og[...]
+    out_copies = []
+    for delta in range(1, n_all):
+        out_copies.append(
+            remote(og, og_r.at[me], osend.at[delta - 1], orecv.at[delta - 1], spot(delta))
+        )
+    sends += out_copies
+    for copy in out_copies:
+        copy.wait_recv()
+    square = jnp.zeros((rows, 1), jnp.float32)
+    for at in range(kv_n):
+        tokens = jnp.concatenate(
+            [tg[at * tp_n + g].astype(jnp.float32) for g in range(tp_n)], axis=1
+        )
+        attention = og_r[at * tp_n].astype(jnp.float32)
+        for g in range(1, tp_n):
+            attention = attention + og_r[at * tp_n + g].astype(jnp.float32)
+        piece = tokens + attention
+        stream[:, at * features:(at + 1) * features] = piece
+        square = square + jnp.sum(piece * piece, axis=1, keepdims=True)
+    scale = lax.rsqrt(square / (n_all * own) + EPS)
+    normed = (stream[...] * scale * mgain[...]).astype(jnp.bfloat16)
+
+    loads[4].wait()
+    loads[5].wait()
+    units = wg.shape[0]
+    step = LANES
+
+    def unit_block(j, carry):
+        at = pl.ds(pl.multiple_of(j * step, step), step)
+        gate = inner_last(normed, wg[at, :])
+        up = inner_last(normed, wu[at, :])
+        hid[:, at] = (gate / (1.0 + jnp.exp(-gate)) * up).astype(jnp.bfloat16)
+        return carry
+
+    lax.fori_loop(0, units // step, unit_block, 0)
+    hidden = hid[...]
+    loads[6].wait()
+    order = [n_all // 2 + (i + 1) // 2 * (1 if i % 2 else -1) for i in range(n_all)]
+    order = [d for d in order if 0 < d < n_all] + [0]
+    down_copies = []
+    mine = None
+    for delta in order:
+        at = lax.rem(me + delta, n_all)
+        block = jnp.dot(
+            hidden,
+            wd[:, pl.ds(pl.multiple_of(at * own, LANES), own)],
+            preferred_element_type=jnp.float32,
+        )
+        if delta == 0:
+            mine = block
+        else:
+            ds[delta - 1] = block
+            down_copies.append(
+                remote(
+                    ds.at[delta - 1], dr.at[delta - 1],
+                    dsend.at[delta - 1], drecv.at[delta - 1], spot(delta),
+                )
+            )
+    sends += down_copies
+    total = mine
+    for copy in down_copies:
+        copy.wait_recv()
+    for delta in range(1, n_all):
+        total = total + dr[delta - 1]
+    mixed = stream[:, pl.ds(pl.multiple_of(me * own, LANES), own)] + total
+    out[...] = mixed.astype(out.dtype)
+    for copy in sends:
+        copy.wait_send()
+
+
+def turning(head_dim, position):
+    half_len = head_dim // 4
+    inv_freq = np.float32(1.0) / np.float32(THETA) ** (
+        np.arange(half_len, dtype=np.float32) / np.float32(half_len)
+    )
+    angles = (np.float32(position) * inv_freq.astype(np.float32)).astype(np.float32)
+    cos, sin = np.cos(angles), np.sin(angles)
+    return np.stack(
+        [np.concatenate([cos, cos] * 2), np.concatenate([-sin, sin] * 2)]
+    ).astype(np.float32)
+
+
+def fused(kv_n, tp_n, *arrays):
+    (tokens, attn_gain, wq, kc, vc, lam, hgain, wo, mgain, wg, wu, wd) = arrays
+    rows, own = tokens.shape
+    n_all = kv_n * tp_n
+    positions, value_dim = kc.shape[1], kc.shape[3]
+    heads = lam.shape[0]
+    both = 2 * heads
+    model = n_all * own
+    f32, bf16 = jnp.float32, jnp.bfloat16
+    table = jnp.asarray(turning(value_dim, positions * kv_n))
+    dma = pltpu.SemaphoreType.DMA
+    vmem = pl.BlockSpec(memory_space=pltpu.VMEM)
+    hbm = pl.BlockSpec(memory_space=pl.ANY)
+    return pl.pallas_call(
+        functools.partial(same_chip_kernel, kv_n, tp_n),
+        out_shape=jax.ShapeDtypeStruct((rows, own), tokens.dtype),
+        in_specs=[vmem, vmem, hbm, hbm, hbm, vmem, vmem, hbm, vmem, hbm, hbm, hbm, vmem],
+        out_specs=vmem,
+        scratch_shapes=[
+            pltpu.VMEM(wq.shape, bf16),
+            pltpu.VMEM((rows, positions, value_dim), bf16),
+            pltpu.VMEM((rows, positions, value_dim), bf16),
+            pltpu.VMEM(wo.shape, bf16),
+            pltpu.VMEM(wg.shape, bf16),
+            pltpu.VMEM(wu.shape, bf16),
+            pltpu.VMEM(wd.shape, bf16),
+            pltpu.VMEM((n_all, rows, own), bf16),
+            pltpu.VMEM((heads, rows, value_dim), f32),
+            pltpu.VMEM((kv_n - 1, heads, rows, value_dim), f32),
+            pltpu.VMEM((heads, rows, value_dim), f32),
+            pltpu.VMEM((rows, both + 8, value_dim), f32),
+            pltpu.VMEM((kv_n - 1, both + 8, value_dim), f32),
+            pltpu.VMEM((heads, value_dim), bf16),
+            pltpu.VMEM((rows, heads, value_dim), bf16),
+            pltpu.VMEM((rows, heads, value_dim), f32),
+            pltpu.VMEM((rows, wo.shape[0]), bf16),
+            pltpu.VMEM((n_all, rows, wo.shape[0]), bf16),
+            pltpu.VMEM((rows, model), f32),
+            pltpu.VMEM((rows, wg.shape[0]), bf16),
+            pltpu.VMEM((n_all - 1, rows, own), f32),
+            pltpu.VMEM((n_all - 1, rows, own), f32),
+            dma((7,)),
+            dma((n_all,)), dma((n_all,)),
+            dma((heads // 4, kv_n - 1)), dma((heads // 4, kv_n - 1)),
+            dma((kv_n - 1,)), dma((kv_n - 1,)),
+            dma((kv_n - 1,)), dma((kv_n - 1,)),
+            dma((n_all - 1,)), dma((n_all - 1,)),
+            dma((n_all - 1,)), dma((n_all - 1,)),
+        ],
+        compiler_params=pltpu.CompilerParams(
+            collective_id=0, has_side_effects=True, vmem_limit_bytes=67043328
+        ),
+    )(
+        tokens, attn_gain.reshape(1, -1), wq,
+        kc.reshape(rows, positions, value_dim), vc.reshape(rows, positions, value_dim),
+        lam.reshape(1, -1), hgain.reshape(1, -1), wo, mgain.reshape(1, -1), wg, wu, wd, table,
+    )
+
+
+def layer(kv_n, tp_n, *arrays):
+    tokens, kc, wg = arrays[0], arrays[3], arrays[9]
+    small = tokens.shape[0] == kv_n and kc.shape[2] == 1 and tp_n == 2
+    if small and tokens.shape[1] % LANES == 0 and wg.shape[0] % LANES == 0:
+        return fused(kv_n, tp_n, *arrays)
+    return shards(*arrays)
+
+
 def solution(mesh):
     placed = (
         P("dp", ("kv", "tp")),
@@ -148,5 +498,6 @@
         P(("kv", "tp"), None),
     )
     return jax.shard_map(
-        shards, mesh=mesh, in_specs=placed, out_specs=P("dp", ("kv", "tp")), check_vma=False
-    )
+        functools.partial(layer, mesh.shape["kv"], mesh.shape["tp"]),
+        mesh=mesh, in_specs=placed, out_specs=P("dp", ("kv", "tp")), check_vma=False
+    )

time: 175 us -> 41.6 us (0.24)
  blocking collectives: 89.4 us -> 0 us
  Pallas kernels: 0 us -> 40 us
  waiting for transfers between devices: 34.3 us -> 0 us
  matrix products: 26.6 us -> 0 us
  between operations: 13.6 us -> 0.01 us
  local copies, waits for them, and re-layouts: 6.98 us -> 1.28 us
  other arithmetic: 3.75 us -> 0 us
    all_gather x5 -> x0, blocking collectives: 70.5 us -> none  [the longest x3 40.2 us: merged(): everything = jax.tree.map(lambda part: lax.all_gather(part, axis), x)]
    pallas_call x0 -> x1, Pallas kernels: none -> 40 us  [fused(): pl.pallas_call(functools.partial(same_chip_kernel, kv_n, tp_n), out_shape...]
    unnamed x2 -> x0, waiting for transfers between devices: 34.3 us -> none
    dot_general x6 -> x0, matrix products: 26.6 us -> none  [the longest x1 12.5 us: shards(): lax.dot_general(down_weight, hidden, (((0,), (1,)), ((), ())), preferred_...]
    psum x1 -> x0, blocking collectives: 19 us -> none  [shards(): lax.psum(jnp.dot(local_cols, query_weight, preferred_element_type=jnp.flo...]
    unnamed x9 -> x1, local copies, waits for them, and re-layouts: 4.29 us -> 1.28 us
  transfers between devices with their start and end apart: 1 -> 0, of which waited for: 1 -> 0; matrix products, arithmetic and copies ran while one was open for 0% -> 0% of each run, Pallas kernels for 0% -> 0%
where the time goes in v1:
time: 41.6 us; the launch traced here: 41.3 us
  Pallas kernels  40 us (96%)
  local copies, waits for them, and re-layouts  1.28 us (3%)
    pallas_call x1, Pallas kernels, fused(): pl.pallas_call(functools.partial(same_chip_kernel, kv_n, tp_n), out_shape...  40 us
    unnamed x1, local copies, waits for them, and re-layouts  1.28 us

profile of v1, /device:TPU:0, one launch (start us, length us, event | category | flops | bytes accessed | tf_op | source)
XLA Modules:
  0.0 41.3 jit_solution(14819680476913009378)
XLA Ops:
  0.0 40.0 %shard_map.127 = bf16[4,512]{1,0:T(4,128)(2,1)} custom-call(bf16[4,512]{1,0:T(4,128)(2,1)} %tok.1, f32[1,4096]{1,0:T(1,128)} %bitcast.8, bf16[1024,2048]{1,0:T(8,128)(2,1)} %wq_h.1, bf16[4,256,128]{2,1,0:T(8,128)(2,1)} %bitcast.6, bf16[4,256,128]{2,1,0:T(8,128)(2,1)} %bitcast.7, f32[1,16]{1,0:T(1,128)} %bitcast.10, f32[1,128]{1,0:T(1,128)} %bitcast.11, ...), custom_call_target="tpu_custom_call" | custom-call | tf_op jit(solution)/shard_map/pallas_call | solution.py:431
  40.1 1.3 %copy.15 = bf16[4,512]{1,0:T(4,128)(2,1)} copy(bf16[4,512]{1,0:T(4,128)(2,1)} %shard_map.127) | data formatting | bytes 8192

commit v2 on v1

--- a/solution.py
+++ b/solution.py
@@ -11,6 +11,7 @@
 EPS = 1e-06
 THETA = 10000.0
 LANES = 128
+CUTS = (5, 13, 22)
 
 
 def merged(x, axis, combine):
@@ -141,9 +142,9 @@
 def same_chip_kernel(
     kv_n, tp_n, tok, again, wq_h, kc_h, vc_h, lam, hgain, wo_h, mgain, wg_h, wu_h, wd_h, table,
     out,
-    wq, kc, vc, wo, wg, wu, wd,
-    tg, qs, qr, qf, ms, mr, hs, ho, hf, og, og_r, stream, hid, ds, dr,
-    wsem, tsend, trecv, qsend, qrecv, msend, mrecv, hsend, hrecv, osend, orecv, dsend, drecv,
+    wq, kc, vc, wo, stage, wgu_t, wd,
+    tg, qs, qr, qf, ms, mb, mr, st, sr, hf, og, og_r, stream, hid, ds, dr,
+    wsem, csem, tsend, trecv, qsend, qrecv, msend, mrecv, hsend, hrecv, osend, orecv, dsend, drecv,
 ):
     kv, tp = lax.axis_index("kv"), lax.axis_index("tp")
     n_all = kv_n * tp_n
@@ -151,11 +152,56 @@
     rows, own = tok.shape
     loads = []
     for slot, (src, dst) in enumerate(
-        [(wq_h, wq), (kc_h, kc), (vc_h, vc), (wo_h, wo), (wg_h, wg), (wu_h, wu), (wd_h, wd)]
+        [(wq_h, wq), (kc_h, kc), (vc_h, vc), (wo_h, wo)]
     ):
         load = pltpu.make_async_copy(src, dst, wsem.at[slot])
         load.start()
         loads.append(load)
+    features = wo.shape[0]
+    units = wg_h.shape[0]
+    per_weight = units // LANES
+    chunks = 2 * per_weight
+    slots = stage.shape[0]
+
+    def chunk_load(weight, i, slot):
+        piece = pl.ds(pl.multiple_of(i * LANES, LANES), LANES)
+        at = i if weight is wg_h else i + per_weight
+        return pltpu.make_async_copy(weight.at[piece], stage.at[slot], csem.at[at])
+
+    for g in range(slots):
+        if g < per_weight:
+            chunk_load(wg_h, g, g).start()
+        else:
+            chunk_load(wu_h, g - per_weight, g).start()
+
+    def turn(low, high):
+        def turn_gate(i, carry):
+            slot = lax.rem(i, slots)
+            chunk_load(wg_h, i, slot).wait()
+            at = pl.ds(pl.multiple_of(i * LANES, LANES), LANES)
+            wgu_t[0, :, at] = stage[slot].T
+
+            @pl.when(i + slots < chunks)
+            def _():
+                chunk_load(wu_h, i + slots - per_weight, slot).start()
+
+            return carry
+
+        def turn_up(i, carry):
+            slot = lax.rem(i + per_weight, slots)
+            chunk_load(wu_h, i, slot).wait()
+            at = pl.ds(pl.multiple_of(i * LANES, LANES), LANES)
+            wgu_t[1, :, at] = stage[slot].T
+            return carry
+
+        low, high = chunks * low // 22, chunks * high // 22
+        if low < per_weight:
+            lax.fori_loop(low, min(high, per_weight), turn_gate, 0)
+        if high > per_weight:
+            lax.fori_loop(max(low, per_weight) - per_weight, high - per_weight, turn_up, 0)
+
+    down_load = pltpu.make_async_copy(wd_h, wd, wsem.at[4])
+    down_load.start()
 
     def spot(delta):
         other = lax.rem(me + delta, n_all)
@@ -229,6 +275,7 @@
         square = square + jnp.sum(wide * wide, axis=1, keepdims=True)
     scale = lax.rsqrt(square / (n_all * own) + EPS)
 
+    turn(0, CUTS[0])
     for copy in query_copies:
         copy.wait_recv()
     lane = lax.broadcasted_iota(jnp.int32, (rows, value_dim), 1)
@@ -254,6 +301,7 @@
     low = lax.broadcasted_iota(jnp.int32, (head_count, value_dim), 1) < half
     row_at = lax.broadcasted_iota(jnp.int32, (both, value_dim), 0)
     lane_at = lax.broadcasted_iota(jnp.int32, (both, value_dim), 1)
+    spread = []
     for b in range(rows):
         query = qf[:, b, :]
         grid = jnp.concatenate(
@@ -263,71 +311,69 @@
         peak = jnp.max(scores, axis=1, keepdims=True)
         exps = jnp.exp(scores - peak)
         sums = jnp.sum(exps, axis=1, keepdims=True)
-        ms[b, 0:both, :] = jnp.dot(
-            exps.astype(jnp.bfloat16), vc[b], preferred_element_type=jnp.float32
-        )
+        spread.append(exps.astype(jnp.bfloat16))
         stats = jnp.where(lane_at == row_at, peak, 0.0) + jnp.where(
             lane_at == row_at + both, sums, 0.0
         )
-        ms[b, both:both + 8, :] = jnp.broadcast_to(
-            jnp.sum(stats, axis=0, keepdims=True), (8, value_dim)
-        )
-
+        st[b:b + 1, :] = jnp.sum(stats, axis=0, keepdims=True)
+    stat_copies = []
+    for delta in range(1, kv_n):
+        stat_copies.append(
+            remote(
+                st, sr.at[delta - 1], hsend.at[delta - 1], hrecv.at[delta - 1], along(delta)
+            )
+        )
     merge_copies = []
-    for delta in range(1, kv_n):
-        other = lax.rem(kv + delta, kv_n)
-        merge_copies.append(
-            remote(
-                ms.at[other], mr.at[delta - 1],
-                msend.at[delta - 1], mrecv.at[delta - 1], along(delta),
+    for b in range(rows):
+        values = jnp.dot(spread[b], vc[b], preferred_element_type=jnp.float32)
+        ms[b] = values
+        mb[b] = values.astype(jnp.bfloat16)
+        for delta in range(1, kv_n):
+            merge_copies.append(
+                remote(
+                    mb.at[b], mr.at[delta - 1, b],
+                    msend.at[b, delta - 1], mrecv.at[b, delta - 1], along(delta),
+                )
             )
-        )
-    sends += merge_copies
+    sends += stat_copies + merge_copies
 
     lam_at = lax.broadcasted_iota(jnp.int32, (head_count, head_count), 0)
     lam_lane = lax.broadcasted_iota(jnp.int32, (head_count, head_count), 1)
     lam_col = jnp.sum(
         jnp.where(lam_at == lam_lane, lam[...], 0.0), axis=1, keepdims=True
     )
-    for copy in merge_copies:
-        copy.wait_recv()
-    gathered = []
-    for source in range(kv_n):
-        block = ms[kv] if source == 0 else mr[source - 1]
-        stats = block[both:both + 1, :]
-        peak = jnp.sum(jnp.where(lane_at == row_at, stats, 0.0), axis=1, keepdims=True)
-        sums = jnp.sum(jnp.where(lane_at == row_at + both, stats, 0.0), axis=1, keepdims=True)
-        gathered.append((peak, sums, block[0:both, :]))
-    top = gathered[0][0]
-    for peak, _, _ in gathered[1:]:
-        top = jnp.maximum(top, peak)
-    all_sums = jnp.zeros_like(top)
-    weighted = jnp.zeros((both, value_dim), jnp.float32)
-    for peak, sums, values in gathered:
-        factor = jnp.exp(peak - top)
-        all_sums = all_sums + sums * factor
-        weighted = weighted + values * factor
-    attended = weighted / all_sums
-    difference = attended[0:head_count] - lam_col * attended[head_count:both]
-    norm = lax.rsqrt(jnp.mean(difference * difference, axis=1, keepdims=True) + EPS)
-    head_out = (difference * norm * hgain[...]).astype(jnp.bfloat16)
-    hs[...] = head_out
-    ho[kv] = head_out
-    head_copies = []
-    for delta in range(1, kv_n):
-        head_copies.append(
-            remote(hs, ho.at[kv], hsend.at[delta - 1], hrecv.at[delta - 1], along(delta))
-        )
-    sends += head_copies
-    for copy in head_copies:
+    turn(CUTS[0], CUTS[1])
+    for copy in stat_copies:
         copy.wait_recv()
     for b in range(rows):
-        hf[b] = ho[b].astype(jnp.float32)
+        for copy in merge_copies[b * (kv_n - 1):(b + 1) * (kv_n - 1)]:
+            copy.wait_recv()
+        gathered = []
+        for source in range(kv_n):
+            stats = st[b:b + 1, :] if source == 0 else sr[source - 1, b:b + 1, :]
+            values = ms[b] if source == 0 else mr[source - 1, b].astype(jnp.float32)
+            peak = jnp.sum(jnp.where(lane_at == row_at, stats, 0.0), axis=1, keepdims=True)
+            sums = jnp.sum(
+                jnp.where(lane_at == row_at + both, stats, 0.0), axis=1, keepdims=True
+            )
+            gathered.append((peak, sums, values))
+        top = gathered[0][0]
+        for peak, _, _ in gathered[1:]:
+            top = jnp.maximum(top, peak)
+        all_sums = jnp.zeros_like(top)
+        weighted = jnp.zeros((both, value_dim), jnp.float32)
+        for peak, sums, values in gathered:
+            factor = jnp.exp(peak - top)
+            all_sums = all_sums + sums * factor
+            weighted = weighted + values * factor
+        attended = weighted / all_sums
+        difference = attended[0:head_count] - lam_col * attended[head_count:both]
+        norm = lax.rsqrt(jnp.mean(difference * difference, axis=1, keepdims=True) + EPS)
+        hf[b] = difference * norm * hgain[...]
     flat = jnp.concatenate(
         [hf[:, h, :] for h in range(head_count)], axis=1
     ).astype(jnp.bfloat16)
     loads[3].wait()
-    features = wo.shape[0]
     width = 256
     for j in range(features // width):
         part = inner_last(flat, wo[j * width:(j + 1) * width, :]).astype(jnp.bfloat16)
@@ -339,6 +385,7 @@
             remote(og, og_r.at[me], osend.at[delta - 1], orecv.at[delta - 1], spot(delta))
         )
     sends += out_copies
+    turn(CUTS[1], CUTS[2])
     for copy in out_copies:
         copy.wait_recv()
     square = jnp.zeros((rows, 1), jnp.float32)
@@ -355,21 +402,14 @@
     scale = lax.rsqrt(square / (n_all * own) + EPS)
     normed = (stream[...] * scale * mgain[...]).astype(jnp.bfloat16)
 
-    loads[4].wait()
-    loads[5].wait()
-    units = wg.shape[0]
-    step = LANES
-
-    def unit_block(j, carry):
-        at = pl.ds(pl.multiple_of(j * step, step), step)
-        gate = inner_last(normed, wg[at, :])
-        up = inner_last(normed, wu[at, :])
+    step = 2 * LANES
+    for low in range(0, units, step):
+        at = slice(low, min(low + step, units))
+        gate = jnp.dot(normed, wgu_t[0, :, at], preferred_element_type=jnp.float32)
+        up = jnp.dot(normed, wgu_t[1, :, at], preferred_element_type=jnp.float32)
         hid[:, at] = (gate / (1.0 + jnp.exp(-gate)) * up).astype(jnp.bfloat16)
-        return carry
-
-    lax.fori_loop(0, units // step, unit_block, 0)
     hidden = hid[...]
-    loads[6].wait()
+    down_load.wait()
     order = [n_all // 2 + (i + 1) // 2 * (1 if i % 2 else -1) for i in range(n_all)]
     order = [d for d in order if 0 < d < n_all] + [0]
     down_copies = []
@@ -384,7 +424,7 @@
         if delta == 0:
             mine = block
         else:
-            ds[delta - 1] = block
+            ds[delta - 1] = block.astype(ds.dtype)
             down_copies.append(
                 remote(
                     ds.at[delta - 1], dr.at[delta - 1],
@@ -396,7 +436,7 @@
     for copy in down_copies:
         copy.wait_recv()
     for delta in range(1, n_all):
-        total = total + dr[delta - 1]
+        total = total + dr[delta - 1].astype(jnp.float32)
     mixed = stream[:, pl.ds(pl.multiple_of(me * own, LANES), own)] + total
     out[...] = mixed.astype(out.dtype)
     for copy in sends:
@@ -423,6 +463,7 @@
     heads = lam.shape[0]
     both = 2 * heads
     model = n_all * own
+    per_weight = wg.shape[0] // LANES
     f32, bf16 = jnp.float32, jnp.bfloat16
     table = jnp.asarray(turning(value_dim, positions * kv_n))
     dma = pltpu.SemaphoreType.DMA
@@ -438,28 +479,29 @@
             pltpu.VMEM((rows, positions, value_dim), bf16),
             pltpu.VMEM((rows, positions, value_dim), bf16),
             pltpu.VMEM(wo.shape, bf16),
-            pltpu.VMEM(wg.shape, bf16),
-            pltpu.VMEM(wu.shape, bf16),
+            pltpu.VMEM((min(per_weight + 5, 2 * per_weight), LANES, model), bf16),
+            pltpu.VMEM((2,) + wg.shape[::-1], bf16),
             pltpu.VMEM(wd.shape, bf16),
             pltpu.VMEM((n_all, rows, own), bf16),
             pltpu.VMEM((heads, rows, value_dim), f32),
             pltpu.VMEM((kv_n - 1, heads, rows, value_dim), f32),
             pltpu.VMEM((heads, rows, value_dim), f32),
-            pltpu.VMEM((rows, both + 8, value_dim), f32),
-            pltpu.VMEM((kv_n - 1, both + 8, value_dim), f32),
-            pltpu.VMEM((heads, value_dim), bf16),
-            pltpu.VMEM((rows, heads, value_dim), bf16),
+            pltpu.VMEM((rows, both, value_dim), f32),
+            pltpu.VMEM((rows, both, value_dim), bf16),
+            pltpu.VMEM((kv_n - 1, rows, both, value_dim), bf16),
+            pltpu.VMEM((rows, value_dim), f32),
+            pltpu.VMEM((kv_n - 1, rows, value_dim), f32),
             pltpu.VMEM((rows, heads, value_dim), f32),
             pltpu.VMEM((rows, wo.shape[0]), bf16),
             pltpu.VMEM((n_all, rows, wo.shape[0]), bf16),
             pltpu.VMEM((rows, model), f32),
             pltpu.VMEM((rows, wg.shape[0]), bf16),
-            pltpu.VMEM((n_all - 1, rows, own), f32),
-            pltpu.VMEM((n_all - 1, rows, own), f32),
-            dma((7,)),
+            pltpu.VMEM((n_all - 1, rows, own), bf16),
+            pltpu.VMEM((n_all - 1, rows, own), bf16),
+            dma((5,)), dma((2 * per_weight,)),
             dma((n_all,)), dma((n_all,)),
             dma((heads // 4, kv_n - 1)), dma((heads // 4, kv_n - 1)),
-            dma((kv_n - 1,)), dma((kv_n - 1,)),
+            dma((rows, kv_n - 1)), dma((rows, kv_n - 1)),
             dma((kv_n - 1,)), dma((kv_n - 1,)),
             dma((n_all - 1,)), dma((n_all - 1,)),
             dma((n_all - 1,)), dma((n_all - 1,)),

time: 41.6 us -> 35.9 us (0.86)
  Pallas kernels: 40 us -> 34.4 us
    pallas_call x1, Pallas kernels: 40 us -> 34.4 us  [fused(): pl.pallas_call(functools.partial(same_chip_kernel, kv_n, tp_n), out_shape...]
where the time goes in v2:
time: 35.9 us; the launch traced here: 35.6 us
  Pallas kernels  34.4 us (96%)
  local copies, waits for them, and re-layouts  1.28 us (4%)
    pallas_call x1, Pallas kernels, fused(): pl.pallas_call(functools.partial(same_chip_kernel, kv_n, tp_n), out_shape...  34.4 us
    unnamed x1, local copies, waits for them, and re-layouts  1.28 us

profile of v2, /device:TPU:0, one launch (start us, length us, event | category | flops | bytes accessed | tf_op | source)
XLA Modules:
  0.0 35.6 jit_solution(13552084557305267635)
XLA Ops:
  0.0 34.4 %shard_map.127 = bf16[4,512]{1,0:T(4,128)(2,1)} custom-call(bf16[4,512]{1,0:T(4,128)(2,1)} %tok.1, f32[1,4096]{1,0:T(1,128)} %bitcast.8, bf16[1024,2048]{1,0:T(8,128)(2,1)} %wq_h.1, bf16[4,256,128]{2,1,0:T(8,128)(2,1)} %bitcast.6, bf16[4,256,128]{2,1,0:T(8,128)(2,1)} %bitcast.7, f32[1,16]{1,0:T(1,128)} %bitcast.10, f32[1,128]{1,0:T(1,128)} %bitcast.11, ...), custom_call_target="tpu_custom_call" | custom-call | tf_op jit(solution)/shard_map/pallas_call | solution.py:472
  34.4 1.3 %copy.15 = bf16[4,512]{1,0:T(4,128)(2,1)} copy(bf16[4,512]{1,0:T(4,128)(2,1)} %shard_map.127) | data formatting | bytes 8192
